TPU v7x, 32 devices: a whole 2x2x4 slice. The times are simulated.
32 devices in a mesh: sp: 8 (over z, y), tp: 4 (over x, core).
Axes of the slice: x: 2, y: 2, z: 4, core: 2. Of those that a mesh axis runs over, the one named last changes fastest.
Arguments:
- stream: bfloat16 [8192, 4096], P('sp', 'tp'), may hold values from -11 to 11
- norm_gain: bfloat16 [3, 4096], P(None, 'tp'), may hold values from 0.099609375 to 1.8984375
- pool_weight: bfloat16 [3, 4, 1024, 1024], P(None, 'tp', 'sp'), may hold values from -0.1875 to 0.1875
- pool_scale: bfloat16 [3, 4096], P(None, 'tp'), may hold values from 0.099609375 to 1.8984375
Outputs:
- mixed: bfloat16 [8192, 4096], P('sp', 'tp')
All inputs are finite; a program needn't handle non-finite values.
Results may differ from a plain program's by a relative error of at most 0.015.
Values may be sent and summed in bfloat16 or wider, within the bound.
A program may use at most 64 MiB of HBM per device.

v0:
```python
import jax
import jax.numpy as jnp
from jax import lax
from jax.sharding import PartitionSpec as P

D = 4096
POOL_GROUPS = 4
norm_eps = 1e-06


def padded(value, sides, width):
    for axis, dim in sides:
        devices, length = (lax.axis_size(axis), value.shape[dim])
        up = [(i, (i + 1) % devices) for i in range(devices - 1)]
        down = [(j, i) for i, j in up]
        last = lax.slice_in_dim(value, length - width, length, axis=dim)
        initial = lax.slice_in_dim(value, 0, width, axis=dim)
        before = lax.ppermute(last, axis, up)
        after = lax.ppermute(initial, axis, down)
        value = jnp.concatenate([before, value, after], axis=dim)
    return value


def window_pool(extended, out_rows, centre, halves, seq_total, reach_rows, per_dev, group_width):
    ext_float = extended.astype(jnp.float32).reshape(extended.shape[0], per_dev, group_width)
    window_sums = jnp.zeros((out_rows, per_dev, group_width), jnp.float32)
    for offset in range(-reach_rows, reach_rows):
        in_window = ((offset >= -halves) & (offset < halves)).astype(jnp.float32)
        window_sums = (
            window_sums
            + ext_float[reach_rows + offset : reach_rows + offset + out_rows]
            * in_window[None, :, None]
        )
    low_end = jnp.maximum(centre[:, None] - halves[None, :], 0)
    high_end = jnp.minimum(centre[:, None] + halves[None, :], seq_total)
    counts = jnp.maximum(high_end - low_end, 1).astype(jnp.float32)
    middle = ext_float[reach_rows : reach_rows + out_rows]
    return (window_sums / counts[:, :, None] - middle).astype(jnp.bfloat16)


def local(stream, norm_gain, pool_weight, pool_scale):
    tok_rows, local_width = stream.shape
    layers, per_dev, shard_rows, group_width = pool_weight.shape
    reach_rows = 2**POOL_GROUPS // 2
    seq_total = tok_rows * lax.axis_size("sp")
    first_pos = lax.axis_index("sp") * tok_rows
    groups = lax.axis_index("tp") * per_dev + jnp.arange(per_dev, dtype=jnp.int32)
    halves = jnp.left_shift(jnp.int32(1), groups)
    deep_rows = reach_rows * layers
    current = padded(stream, (("sp", 0),), deep_rows)
    base_pos = first_pos - deep_rows
    for layer_idx in range(layers):
        ext_rows = current.shape[0]
        positions = base_pos + jnp.arange(ext_rows, dtype=jnp.int32)
        inside = (positions >= 0) & (positions < seq_total)
        current_f = current.astype(jnp.float32)
        square_sums = lax.psum(jnp.sum(current_f * current_f, axis=1), "tp")
        row_scale = lax.rsqrt(square_sums / D + norm_eps)
        normed = current_f * row_scale[:, None] * norm_gain[layer_idx].astype(jnp.float32)
        normed = jnp.where(inside[:, None], normed, 0.0).astype(jnp.bfloat16)
        out_rows = ext_rows - 2 * reach_rows
        residual = current_f[reach_rows : ext_rows - reach_rows]
        centre = positions[reach_rows : ext_rows - reach_rows]
        base_pos = base_pos + reach_rows
        pooled = window_pool(
            normed, out_rows, centre, halves, seq_total, reach_rows, per_dev, group_width
        )
        branch = jnp.einsum(
            "tgc,gcd->tgd",
            pooled,
            lax.all_gather(pool_weight[layer_idx], "sp", axis=1, tiled=True),
            preferred_element_type=jnp.float32,
        )
        branch = branch.reshape(out_rows, local_width)
        current = (residual + branch * pool_scale[layer_idx].astype(jnp.float32)).astype(
            jnp.bfloat16
        )
    return current


def solution(mesh):
    placed = (P("sp", "tp"), P(None, "tp"), P(None, "tp", "sp", None), P(None, "tp"))
    return jax.shard_map(
        local, mesh=mesh, in_specs=placed, out_specs=P("sp", "tp"), check_vma=False
    )
```

profile of v0, /device:TPU:0, one launch (start us, length us, event | category | flops | bytes accessed | tf_op | source)
XLA Modules:
  0.0 213.5 jit_solution(14513719529926578591)
XLA Ops:
  6.5 0.0 copy-start
  6.5 0.0 all-gather.7.cloned.1.call-start
  6.5 2.2 %fusion.70 = (bf16[1,1,128,1024]{3,2,1,0:T(8,128)(2,1)}, bf16[1,1,128,1024]{3,2,1,0:T(8,128)(2,1)}, bf16[1,1,128,1024]{3,2,1,0:T(8,128)(2,1)}) fusion(bf16[3,1,128,1024]{3,2,1,0:T(8,128)(2,1)} %param.6), kind=kLoop, calls=%fused_computation.141 | loop fusion | bytes 1572864 | tf_op jit(solution)/shard_map/slice | solution.py:71
  8.7 0.0 all-gather.7.cloned.1.call-update
  8.7 0.0 all-gather.9.cloned.1.call-start
  8.8 0.7 all-gather.9.cloned.1.call-update
  9.5 0.0 all-gather.11.cloned.1.call-start
  9.5 0.8 fusion.69
  10.4 4.9 %collective-permute-start = (bf16[24,1024]{1,0:T(8,128)(2,1)S(1)}, bf16[24,1024]{1,0:T(8,128)(2,1)S(1)}, u32[]{:S(2)}, u32[]{:S(2)}) collective-permute-start(bf16[24,1024]{1,0:T(8,128)(2,1)S(1)} %get-tuple-element.5), channel_id=1, source_target_pairs={{0,4},{4,8},{8,12},{12,16},{16,20},{20,24},{24,28},{1,5},{5,9},{9,... | collective-permute-start | bytes 147464 | tf_op jit(solution)/shard_map/ppermute | solution.py:18
  15.3 1.3 collective-permute-start.1
  16.6 0.0 all-gather.11.cloned.1.call-update
  16.6 0.8 slice_convert_fusion.1
  17.5 0.8 slice_convert_fusion
  18.3 0.1 maximum_convert_fusion.2
  18.4 0.1 maximum_convert_fusion.1
  18.5 0.1 maximum_convert_fusion.3
  18.7 0.0 collective-permute-done
  18.7 2.5 %collective-permute-done.1 = bf16[24,1024]{1,0:T(8,128)(2,1)S(1)} collective-permute-done((bf16[24,1024]{1,0:T(8,128)(2,1)S(1)}, bf16[24,1024]{1,0:T(8,128)(2,1)S(1)}, u32[]{:S(2)}, u32[]{:S(2)}) %collective-permute-start.1) | collective-permute-done | bytes 49184 | tf_op jit(solution)/shard_map/ppermute | solution.py:19
  21.2 0.0 copy-done
  21.2 0.5 multiply_reduce_fusion
  21.8 6.2 %psum.21 = f32[1072]{0:T(1024)S(1)} all-reduce(f32[1072]{0:T(1024)S(1)} %multiply_reduce_fusion), channel_id=1, replica_groups=mesh['sp'=8,'tp'=4] {'tp'}, use_global_device_ids=true, to_apply=%region_1.0 | all-reduce | flops 1072 | bytes 8576 | tf_op jit(solution)/shard_map/psum | solution.py:57
  27.9 2.5 %maximum_convert_fusion = f32[1072,1024]{1,0:T(8,128)} fusion(bf16[24,1024]{1,0:T(8,128)(2,1)S(1)} %collective-permute-done.1, bf16[1024,1024]{1,0:T(8,128)(2,1)S(1)} %copy-done, bf16[24,1024]{1,0:T(8,128)(2,1)S(1)} %collective-permute-done), kind=kLoop, calls=%fused_computation.115 | loop fusion | flops 6586368 | bytes 6586368 | tf_op jit(solution)/shard_map/convert_element_type | solution.py:56
  30.5 2.9 %fusion.59 = f32[1072,1024]{1,0:T(8,128)} fusion(f32[1024]{0:T(1024)S(1)} %bitcast.21, f32[1072]{0:T(1024)S(1)} %add_rsqrt_fusion.2, pred[1072]{0:T(1024)(128)(4,1)S(1)} %compare_and_fusion.2, bf16[24,1024]{1,0:T(8,128)(2,1)S(1)} %collective-permute-done.1, bf16[1024,1024]{1,0:T(8,128)(2,1)S(1)} %copy-done, bf16[24,1024]{1,0:T(8,128)(2,1)S(1)} %collective-permute-done), kind=kLoop, calls=%fused_computation.114 | loop fusion | flops 12075008 | bytes 6595824 | tf_op jit(solution)/shard_map/convert_element_type | solution.py:25
  33.4 28.0 %all-gather.7.cloned.1.call-done = bf16[1,1,1024,1024]{3,2,1,0:T(8,128)(2,1)} async-done(((bf16[1,1,128,1024]{3,2,1,0:T(8,128)(2,1)}), bf16[1,1,1024,1024]{3,2,1,0:T(8,128)(2,1)}) %all-gather.7.cloned.1.call-update) | async-done | bytes 2097168 | tf_op jit(solution)/shard_map/all_gather | solution.py:71
  61.4 42.3 %multiply_reduce_fusion.1 = (f32[1056]{0:T(1024)S(1)}, f32[1056,1024]{1,0:T(8,128)}) fusion(f32[1024]{0:T(1024)S(1)} %bitcast.24, bf16[1,1,1024,1024]{3,2,1,0:T(8,128)(2,1)} %all-gather.7.cloned.1.call-done, f32[1072,1024]{1,0:T(8,128)} %fusion.59, f32[1056]{0:T(1024)S(1)} %maximum_convert_fusion.2, f32[]{:T(128)S(6)} %mul.631, f32[]{:T(128)S(6)} %mul.628, ...), kind=kOutput, calls=%fused_computation.40 | convolution fusion | flops 2257845248 | bytes 79966528 | tf_op jit(solution)/shard_map/tgc,gcd->tgd/dot_general | solution.py:68
  103.7 6.3 %psum.22 = f32[1056]{0:T(1024)S(1)} all-reduce(f32[1056]{0:T(1024)S(1)} %get-tuple-element.16), channel_id=1, replica_groups=mesh['sp'=8,'tp'=4] {'tp'}, use_global_device_ids=true, to_apply=%region_3.4 | all-reduce | flops 1056 | bytes 8448 | tf_op jit(solution)/shard_map/psum | solution.py:57
  110.0 4.7 %fusion.60 = f32[1056,1024]{1,0:T(8,128)} fusion(f32[1056,1024]{1,0:T(8,128)} %get-tuple-element.17, f32[1024]{0:T(1024)S(1)} %bitcast.20, f32[1056]{0:T(1024)S(1)} %add_rsqrt_fusion.1, pred[1056]{0:T(1024)(128)(4,1)S(1)} %compare_and_fusion.1), kind=kLoop, calls=%fused_computation.116 | loop fusion | flops 5406720 | bytes 8660128 | tf_op jit(solution)/shard_map/convert_element_type | solution.py:25
  114.8 0.0 all-gather.9.cloned.1.call-done
  114.8 41.7 %multiply_reduce_fusion.2 = (f32[1040]{0:T(1024)S(1)}, f32[1040,1024]{1,0:T(8,128)}) fusion(f32[1024]{0:T(1024)S(1)} %bitcast.23, bf16[1,1,1024,1024]{3,2,1,0:T(8,128)(2,1)} %all-gather.9.cloned.1.call-done, f32[1056,1024]{1,0:T(8,128)} %fusion.60, f32[1040]{0:T(1024)S(1)} %maximum_convert_fusion.1, f32[]{:T(128)S(6)} %mul.631, f32[]{:T(128)S(6)} %mul.628, ...), kind=kOutput, calls=%fused_computation.75 | convolution fusion | flops 2223635456 | bytes 78786752 | tf_op jit(solution)/shard_map/tgc,gcd->tgd/dot_general | solution.py:68
  156.4 6.7 %psum.23 = f32[1040]{0:T(1024)S(1)} all-reduce(f32[1040]{0:T(1024)S(1)} %get-tuple-element.18), channel_id=1, replica_groups=mesh['sp'=8,'tp'=4] {'tp'}, use_global_device_ids=true, to_apply=%region_5.6 | all-reduce | flops 1040 | bytes 8320 | tf_op jit(solution)/shard_map/psum | solution.py:57
  163.1 4.7 %fusion.63 = f32[1040,1024]{1,0:T(8,128)} fusion(f32[1040,1024]{1,0:T(8,128)} %get-tuple-element.19, f32[1024]{0:T(1024)S(1)} %bitcast.19, f32[1040]{0:T(1024)S(1)} %add_rsqrt_fusion, pred[1040]{0:T(1024)(128)(4,1)S(1)} %compare_and_fusion), kind=kLoop, calls=%fused_computation.118 | loop fusion | flops 5324800 | bytes 8528976 | tf_op jit(solution)/shard_map/convert_element_type | solution.py:25
  167.8 39.2 %fusion.55 = bf16[1024,1024]{1,0:T(8,128)(2,1)} fusion(f32[1040,1024]{1,0:T(8,128)} %get-tuple-element.19, bf16[1,1,1024,1024]{3,2,1,0:T(8,128)(2,1)} %all-gather.11.cloned.1.call-done, f32[1024]{0:T(1024)S(1)} %bitcast.22, f32[1040,1024]{1,0:T(8,128)} %fusion.63, f32[1024]{0:T(1024)S(1)} %maximum_convert_fusion.3, f32[]{:T(128)S(6)} %mul.631, ...), kind=kOutput, calls=%fused_computation.110 | convolution fusion | flops 2186280960 | bytes 75505728 | tf_op jit(solution)/shard_map/tgc,gcd->tgd/dot_general | solution.py:68
  (10 shorter events, 0.1 us)
Async XLA Ops:
  6.5 14.7 %copy-start = (bf16[1024,1024]{1,0:T(8,128)(2,1)S(1)}, bf16[1024,1024]{1,0:T(8,128)(2,1)}, u32[]{:S(2)}) copy-start(bf16[1024,1024]{1,0:T(8,128)(2,1)} %param.4) | copy-start | bytes 6291460
  6.5 54.9 %all-gather.7.cloned.1.call-start = ((), (), s32[]{:S(2)}) async-start(), calls=%async_computation | async-start | bytes 2359296 | tf_op jit(solution)/shard_map/all_gather | solution.py:71
  8.7 106.1 %all-gather.9.cloned.1.call-start = ((), (), s32[]{:S(2)}) async-start(), calls=%async_computation.1 | async-start | bytes 2359296 | tf_op jit(solution)/shard_map/all_gather | solution.py:71
  9.5 158.3 %all-gather.11.cloned.1.call-start = ((), (), s32[]{:S(2)}) async-start(), calls=%async_computation.2 | async-start | bytes 2359296 | tf_op jit(solution)/shard_map/all_gather | solution.py:71
  10.4 8.3 %collective-permute-start = (bf16[24,1024]{1,0:T(8,128)(2,1)S(1)}, bf16[24,1024]{1,0:T(8,128)(2,1)S(1)}, u32[]{:S(2)}, u32[]{:S(2)}) collective-permute-start(bf16[24,1024]{1,0:T(8,128)(2,1)S(1)} %get-tuple-element.5), channel_id=1, source_target_pairs={{0,4},{4,8},{8,12},{12,16},{16,20},{20,24},{24,28},{1,5},{5,9},{9,... | collective-permute-start | bytes 147464 | tf_op jit(solution)/shard_map/ppermute | solution.py:18
  15.3 6.0 %collective-permute-start.1 = (bf16[24,1024]{1,0:T(8,128)(2,1)S(1)}, bf16[24,1024]{1,0:T(8,128)(2,1)S(1)}, u32[]{:S(2)}, u32[]{:S(2)}) collective-permute-start(bf16[24,1024]{1,0:T(8,128)(2,1)S(1)} %get-tuple-element.6), channel_id=1, source_target_pairs={{4,0},{8,4},{12,8},{16,12},{20,16},{24,20},{28,24},{5,1},{9,5},{13... | collective-permute-start | bytes 147464 | tf_op jit(solution)/shard_map/ppermute | solution.py:19
Sparse Core Ops, SparseCore 0:
  9.5 51.8 all-gather.6
  63.5 47.6 all-gather.8
  113.3 47.6 all-gather.10
where the time goes:
time: 214 us
  matrix products  123 us (57%)
  waiting for transfers between devices  31.3 us (15%)
  blocking collectives  19.2 us (9%)
  other arithmetic  17.3 us (8%)
  between operations  13.4 us (6%)
  starting transfers between devices  6.26 us (3%)
  local copies, waits for them, and re-layouts  3 us (1%)
    dot_general x3, matrix products, local(): jnp.einsum('tgc,gcd->tgd', pooled, lax.all_gather(pool_weight[layer_idx],...  123 us
    all_gather x3, waiting for transfers between devices, local(): lax.all_gather(pool_weight[layer_idx], 'sp', axis=1, tiled=True)  28 us
    psum x3, blocking collectives, local(): square_sums = lax.psum(jnp.sum(current_f * current_f, axis=1), 'tp')  19.2 us
    convert_element_type x3, other arithmetic, window_pool(): extended.astype(jnp.float32)  12.3 us
    ppermute x1, starting transfers between devices, padded(): before = lax.ppermute(last, axis, up)  4.89 us
  transfers between devices with their start and end apart: 5, of which 2 were waited for; matrix products, arithmetic and copies ran while one was open for 48% of the time, Pallas kernels for 0%

commit v1 on v0

--- a/solution.py
+++ b/solution.py
@@ -68,7 +68,7 @@
         branch = jnp.einsum(
             "tgc,gcd->tgd",
             pooled,
-            lax.all_gather(pool_weight[layer_idx], "sp", axis=1, tiled=True),
+            jnp.concatenate(lax.all_gather(pool_weight[layer_idx], "sp"), axis=1),
             preferred_element_type=jnp.float32,
         )
         branch = branch.reshape(out_rows, local_width)

time: 214 us -> 214 us (level)
  no operation moved by 1% of the time
where the time goes in v1:
time: 214 us
  matrix products  123 us (57%)
  waiting for transfers between devices  31.3 us (15%)
  blocking collectives  19.2 us (9%)
  other arithmetic  17.3 us (8%)
  between operations  13.4 us (6%)
  starting transfers between devices  6.26 us (3%)
  local copies, waits for them, and re-layouts  3 us (1%)
    dot_general x3, matrix products, local(): jnp.einsum('tgc,gcd->tgd', pooled, jnp.concatenate(lax.all_gather(pool_we...  123 us
    all_gather x3, waiting for transfers between devices, local(): lax.all_gather(pool_weight[layer_idx], 'sp')  28 us
    psum x3, blocking collectives, local(): square_sums = lax.psum(jnp.sum(current_f * current_f, axis=1), 'tp')  19.2 us
    convert_element_type x3, other arithmetic, window_pool(): extended.astype(jnp.float32)  12.3 us
    ppermute x1, starting transfers between devices, padded(): before = lax.ppermute(last, axis, up)  4.89 us
  transfers between devices with their start and end apart: 5, of which 2 were waited for; matrix products, arithmetic and copies ran while one was open for 48% of the time, Pallas kernels for 0%

profile of v1, /device:TPU:0, one launch (start us, length us, event | category | flops | bytes accessed | tf_op | source)
XLA Modules:
  0.0 213.5 jit_solution(14513719529926578591)
XLA Ops:
  6.5 0.0 copy-start
  6.5 0.0 all-gather.4.cloned.1.call-start
  6.5 2.2 %fusion.67 = (bf16[1,1,128,1024]{3,2,1,0:T(8,128)(2,1)}, bf16[1,1,128,1024]{3,2,1,0:T(8,128)(2,1)}, bf16[1,1,128,1024]{3,2,1,0:T(8,128)(2,1)}) fusion(bf16[3,1,128,1024]{3,2,1,0:T(8,128)(2,1)} %param.6), kind=kLoop, calls=%fused_computation.138 | loop fusion | bytes 1572864 | tf_op jit(solution)/shard_map/slice | solution.py:71
  8.7 0.0 all-gather.4.cloned.1.call-update
  8.7 0.0 all-gather.6.cloned.1.call-start
  8.8 0.7 all-gather.6.cloned.1.call-update
  9.5 0.0 all-gather.8.cloned.1.call-start
  9.5 0.8 fusion.66
  10.4 4.9 %collective-permute-start = (bf16[24,1024]{1,0:T(8,128)(2,1)S(1)}, bf16[24,1024]{1,0:T(8,128)(2,1)S(1)}, u32[]{:S(2)}, u32[]{:S(2)}) collective-permute-start(bf16[24,1024]{1,0:T(8,128)(2,1)S(1)} %get-tuple-element.5), channel_id=1, source_target_pairs={{0,4},{4,8},{8,12},{12,16},{16,20},{20,24},{24,28},{1,5},{5,9},{9,... | collective-permute-start | bytes 147464 | tf_op jit(solution)/shard_map/ppermute | solution.py:18
  15.3 1.3 collective-permute-start.1
  16.6 0.0 all-gather.8.cloned.1.call-update
  16.6 0.8 slice_convert_fusion.1
  17.5 0.8 slice_convert_fusion
  18.3 0.1 maximum_convert_fusion.2
  18.4 0.1 maximum_convert_fusion.1
  18.5 0.1 maximum_convert_fusion.3
  18.7 0.0 collective-permute-done
  18.7 2.5 %collective-permute-done.1 = bf16[24,1024]{1,0:T(8,128)(2,1)S(1)} collective-permute-done((bf16[24,1024]{1,0:T(8,128)(2,1)S(1)}, bf16[24,1024]{1,0:T(8,128)(2,1)S(1)}, u32[]{:S(2)}, u32[]{:S(2)}) %collective-permute-start.1) | collective-permute-done | bytes 49184 | tf_op jit(solution)/shard_map/ppermute | solution.py:19
  21.2 0.0 copy-done
  21.2 0.5 multiply_reduce_fusion
  21.8 6.2 %psum.21 = f32[1072]{0:T(1024)S(1)} all-reduce(f32[1072]{0:T(1024)S(1)} %multiply_reduce_fusion), channel_id=1, replica_groups=mesh['sp'=8,'tp'=4] {'tp'}, use_global_device_ids=true, to_apply=%region_1.0 | all-reduce | flops 1072 | bytes 8576 | tf_op jit(solution)/shard_map/psum | solution.py:57
  27.9 2.5 %maximum_convert_fusion = f32[1072,1024]{1,0:T(8,128)} fusion(bf16[24,1024]{1,0:T(8,128)(2,1)S(1)} %collective-permute-done.1, bf16[1024,1024]{1,0:T(8,128)(2,1)S(1)} %copy-done, bf16[24,1024]{1,0:T(8,128)(2,1)S(1)} %collective-permute-done), kind=kLoop, calls=%fused_computation.115 | loop fusion | flops 6586368 | bytes 6586368 | tf_op jit(solution)/shard_map/convert_element_type | solution.py:56
  30.5 2.9 %fusion.59 = f32[1072,1024]{1,0:T(8,128)} fusion(f32[1024]{0:T(1024)S(1)} %bitcast.14, f32[1072]{0:T(1024)S(1)} %add_rsqrt_fusion.2, pred[1072]{0:T(1024)(128)(4,1)S(1)} %compare_and_fusion.2, bf16[24,1024]{1,0:T(8,128)(2,1)S(1)} %collective-permute-done.1, bf16[1024,1024]{1,0:T(8,128)(2,1)S(1)} %copy-done, bf16[24,1024]{1,0:T(8,128)(2,1)S(1)} %collective-permute-done), kind=kLoop, calls=%fused_computation.114 | loop fusion | flops 12075008 | bytes 6595824 | tf_op jit(solution)/shard_map/convert_element_type | solution.py:25
  33.4 28.0 %all-gather.4.cloned.1.call-done = bf16[8,1,128,1024]{3,2,1,0:T(8,128)(2,1)} async-done(((bf16[1,1,128,1024]{3,2,1,0:T(8,128)(2,1)}), bf16[8,1,128,1024]{3,2,1,0:T(8,128)(2,1)}) %all-gather.4.cloned.1.call-update) | async-done | bytes 2097168 | tf_op jit(solution)/shard_map/all_gather | solution.py:71
  61.4 42.3 %multiply_reduce_fusion.1 = (f32[1056]{0:T(1024)S(1)}, f32[1056,1024]{1,0:T(8,128)}) fusion(f32[1024]{0:T(1024)S(1)} %bitcast.17, bf16[1024,1024]{1,0:T(8,128)(2,1)} %bitcast.20, f32[1072,1024]{1,0:T(8,128)} %fusion.59, f32[1056]{0:T(1024)S(1)} %maximum_convert_fusion.2, f32[]{:T(128)S(6)} %mul.631, f32[]{:T(128)S(6)} %mul.628, f32[]{:T(128)S(6)} %mul.625, ...), kind=kOutput, calls=%fused_computation.40 | convolution fusion | flops 2257845248 | bytes 79966528 | tf_op jit(solution)/shard_map/tgc,gcd->tgd/dot_general | solution.py:68
  103.7 6.3 %psum.22 = f32[1056]{0:T(1024)S(1)} all-reduce(f32[1056]{0:T(1024)S(1)} %get-tuple-element.16), channel_id=1, replica_groups=mesh['sp'=8,'tp'=4] {'tp'}, use_global_device_ids=true, to_apply=%region_3.4 | all-reduce | flops 1056 | bytes 8448 | tf_op jit(solution)/shard_map/psum | solution.py:57
  110.0 4.7 %fusion.60 = f32[1056,1024]{1,0:T(8,128)} fusion(f32[1056,1024]{1,0:T(8,128)} %get-tuple-element.17, f32[1024]{0:T(1024)S(1)} %bitcast.13, f32[1056]{0:T(1024)S(1)} %add_rsqrt_fusion.1, pred[1056]{0:T(1024)(128)(4,1)S(1)} %compare_and_fusion.1), kind=kLoop, calls=%fused_computation.116 | loop fusion | flops 5406720 | bytes 8660128 | tf_op jit(solution)/shard_map/convert_element_type | solution.py:25
  114.8 0.0 all-gather.6.cloned.1.call-done
  114.8 41.7 %multiply_reduce_fusion.2 = (f32[1040]{0:T(1024)S(1)}, f32[1040,1024]{1,0:T(8,128)}) fusion(f32[1024]{0:T(1024)S(1)} %bitcast.16, bf16[1024,1024]{1,0:T(8,128)(2,1)} %bitcast.18, f32[1056,1024]{1,0:T(8,128)} %fusion.60, f32[1040]{0:T(1024)S(1)} %maximum_convert_fusion.1, f32[]{:T(128)S(6)} %mul.631, f32[]{:T(128)S(6)} %mul.628, f32[]{:T(128)S(6)} %mul.625, ...), kind=kOutput, calls=%fused_computation.75 | convolution fusion | flops 2223635456 | bytes 78786752 | tf_op jit(solution)/shard_map/tgc,gcd->tgd/dot_general | solution.py:68
  156.4 6.7 %psum.23 = f32[1040]{0:T(1024)S(1)} all-reduce(f32[1040]{0:T(1024)S(1)} %get-tuple-element.18), channel_id=1, replica_groups=mesh['sp'=8,'tp'=4] {'tp'}, use_global_device_ids=true, to_apply=%region_5.6 | all-reduce | flops 1040 | bytes 8320 | tf_op jit(solution)/shard_map/psum | solution.py:57
  163.1 4.7 %fusion.63 = f32[1040,1024]{1,0:T(8,128)} fusion(f32[1040,1024]{1,0:T(8,128)} %get-tuple-element.19, f32[1024]{0:T(1024)S(1)} %bitcast.12, f32[1040]{0:T(1024)S(1)} %add_rsqrt_fusion, pred[1040]{0:T(1024)(128)(4,1)S(1)} %compare_and_fusion), kind=kLoop, calls=%fused_computation.118 | loop fusion | flops 5324800 | bytes 8528976 | tf_op jit(solution)/shard_map/convert_element_type | solution.py:25
  167.8 39.2 %fusion.55 = bf16[1024,1024]{1,0:T(8,128)(2,1)} fusion(f32[1040,1024]{1,0:T(8,128)} %get-tuple-element.19, bf16[1024,1024]{1,0:T(8,128)(2,1)} %bitcast.19, f32[1024]{0:T(1024)S(1)} %bitcast.15, f32[1040,1024]{1,0:T(8,128)} %fusion.63, f32[1024]{0:T(1024)S(1)} %maximum_convert_fusion.3, f32[]{:T(128)S(6)} %mul.631, f32[]{:T(128)S(6)} %mul.628, ...), kind=kOutput, calls=%fused_computation.110 | convolution fusion | flops 2186280960 | bytes 75505728 | tf_op jit(solution)/shard_map/tgc,gcd->tgd/dot_general | solution.py:68
  (10 shorter events, 0.1 us)
Async XLA Ops:
  6.5 14.7 %copy-start = (bf16[1024,1024]{1,0:T(8,128)(2,1)S(1)}, bf16[1024,1024]{1,0:T(8,128)(2,1)}, u32[]{:S(2)}) copy-start(bf16[1024,1024]{1,0:T(8,128)(2,1)} %param.4) | copy-start | bytes 6291460
  6.5 54.9 %all-gather.4.cloned.1.call-start = ((), (), s32[]{:S(2)}) async-start(), calls=%async_computation | async-start | bytes 2359296 | tf_op jit(solution)/shard_map/all_gather | solution.py:71
  8.7 106.1 %all-gather.6.cloned.1.call-start = ((), (), s32[]{:S(2)}) async-start(), calls=%async_computation.1 | async-start | bytes 2359296 | tf_op jit(solution)/shard_map/all_gather | solution.py:71
  9.5 158.3 %all-gather.8.cloned.1.call-start = ((), (), s32[]{:S(2)}) async-start(), calls=%async_computation.2 | async-start | bytes 2359296 | tf_op jit(solution)/shard_map/all_gather | solution.py:71
  10.4 8.3 %collective-permute-start = (bf16[24,1024]{1,0:T(8,128)(2,1)S(1)}, bf16[24,1024]{1,0:T(8,128)(2,1)S(1)}, u32[]{:S(2)}, u32[]{:S(2)}) collective-permute-start(bf16[24,1024]{1,0:T(8,128)(2,1)S(1)} %get-tuple-element.5), channel_id=1, source_target_pairs={{0,4},{4,8},{8,12},{12,16},{16,20},{20,24},{24,28},{1,5},{5,9},{9,... | collective-permute-start | bytes 147464 | tf_op jit(solution)/shard_map/ppermute | solution.py:18
  15.3 6.0 %collective-permute-start.1 = (bf16[24,1024]{1,0:T(8,128)(2,1)S(1)}, bf16[24,1024]{1,0:T(8,128)(2,1)S(1)}, u32[]{:S(2)}, u32[]{:S(2)}) collective-permute-start(bf16[24,1024]{1,0:T(8,128)(2,1)S(1)} %get-tuple-element.6), channel_id=1, source_target_pairs={{4,0},{8,4},{12,8},{16,12},{20,16},{24,20},{28,24},{5,1},{9,5},{13... | collective-permute-start | bytes 147464 | tf_op jit(solution)/shard_map/ppermute | solution.py:19
Sparse Core Ops, SparseCore 0:
  9.5 51.8 all-gather.3
  63.5 47.6 all-gather.5
  113.3 47.6 all-gather.7
